TPU v7x, 512 devices: a whole 4x8x8 slice. The times are simulated.
512 devices in a mesh: sp: 128 (over z, y, core), tp: 4 (over x).
Axes of the slice: x: 4, y: 8, z: 8, core: 2. Of those that a mesh axis runs over, the one named last changes fastest.
Arguments:
- stream: bfloat16 [32768, 2048], P('sp', 'tp'), may hold values from -6 to 6
- norm_gain: float32 [2, 2048], replicated, may hold values from 0.1 to 1.9
- w_value: bfloat16 [2, 2048, 1024], P(None, 'sp', 'tp'), may hold values from -0.125 to 0.125
- w_gate: bfloat16 [2, 2048, 1024], P(None, 'sp', 'tp'), may hold values from -0.125 to 0.125
- conv_taps: float32 [2, 128, 1024], P(None, None, 'tp'), as said below
- channel_gain: float32 [2, 1024], P(None, 'tp'), may hold values from 0.1 to 1.9
- w_out: bfloat16 [2, 1024, 2048], P(None, 'tp', 'sp'), may hold values from -0.1875 to 0.1875
Outputs:
- result: bfloat16 [32768, 2048], P('sp', 'tp')
Inputs may be any that keep to these rules, and one draw needn't show every extreme that they name: `conv_taps`: taps of each block of 128 consecutive channels share a scale factor of its own.
All inputs are finite; a program needn't handle non-finite values.
Results may differ from a plain program's by a relative error of at most 0.012.
Values may be sent and summed in bfloat16 or wider, within the bound.
No kernel may reach another device: no remote copies, remote signals or barrier semaphores. Data moves between devices by JAX's collectives and lax.ppermute only.
A program may use at most 64 MiB of HBM per device.

v0:
```python
import jax
import jax.numpy as jnp
from jax import lax
from jax.sharding import Mesh
from jax.sharding import PartitionSpec as P

C = 1024
LAYERS = 2
SP = ("sp_0", "sp_1", "sp_2")


def laid_out(parts, dim):
    parts = jnp.moveaxis(parts, 0, dim)
    lengths = parts.shape
    return parts.reshape(*lengths[:dim], lengths[dim] * lengths[dim + 1], *lengths[dim + 2 :])


def sent_to_all(shard, axis):
    copies = jnp.broadcast_to(shard, (lax.axis_size(axis), *shard.shape))
    return lax.all_to_all(copies, axis, split_axis=0, concat_axis=0, tiled=True)


def collect(shard, axis, dim):
    return laid_out(sent_to_all(shard, axis), dim)


def in_one_piece(arrays, axis, dim, along):
    both = jnp.concatenate(arrays, axis=along)
    whole, at, done = (lax.all_gather(both, axis, axis=dim, tiled=True), 0, [])
    for a in arrays:
        done.append(lax.slice_in_dim(whole, at, at + a.shape[along], axis=along))
        at += a.shape[along]
    return tuple(done)


def from_behind(value, axis, steps):
    count = lax.axis_size(axis)
    initial, last = (max(0, -steps), min(count, count - steps))
    return lax.ppermute(value, axis, [(source, source + steps) for source in range(initial, last)])


def of_everyone(shard, axis):
    return sent_to_all(shard, axis).sum(axis=0)


def stacked_from(shard, axes, turns):
    parts = shard[None]
    for k in turns:
        parts = lax.all_gather(parts, axes[k], axis=0, tiled=True)
    held = [lax.axis_size(axes[k]) for k in reversed(turns)]
    parts = parts.reshape(*held, *shard.shape)
    turned = sorted(range(len(turns)), key=lambda place: turns[len(turns) - 1 - place])
    return parts.transpose(*turned, *range(len(turns), parts.ndim)).reshape(-1, *shard.shape)


def gathered_by_axis(shard, axes, turns, dim):
    return laid_out(stacked_from(shard, axes, turns), dim)


def split_up(shard, dim, size):
    lengths = shard.shape
    parts = shard.reshape(*lengths[:dim], size, lengths[dim] // size, *lengths[dim + 1 :])
    return jnp.moveaxis(parts, dim, 0)


def sum_at_owner(shard, axis, dim):
    parts = split_up(shard, dim, lax.axis_size(axis))
    arrived = lax.all_to_all(parts, axis, split_axis=0, concat_axis=0, tiled=True)
    return arrived.astype(jnp.float32).sum(axis=0)


def shards(stream, norm_gain, w_value, w_gate, conv_taps, channel_gain, w_out):
    x = stream
    tokens_here = stream.shape[0]
    local_ch = w_value.shape[2]
    taps = conv_taps.shape[1]
    for layer in range(LAYERS):
        whole = collect(x, "tp", 1).astype(jnp.float32)
        normed = (
            whole
            * lax.rsqrt(jnp.mean(whole * whole, axis=1, keepdims=True) + 1e-06)
            * norm_gain[layer]
        ).astype(jnp.bfloat16)
        value_whole, gate_whole = in_one_piece((w_value[layer], w_gate[layer]), SP, 0, 1)
        value = jnp.dot(normed, value_whole, preferred_element_type=jnp.float32)
        gate = jnp.dot(normed, gate_whole, preferred_element_type=jnp.float32)
        glu = (value * jax.nn.sigmoid(gate)).astype(jnp.bfloat16)
        before = from_behind(glu[tokens_here - taps :], SP, 1)
        padded = jnp.concatenate([before[1:], glu], axis=0).astype(jnp.float32)
        conv = lax.conv_general_dilated(
            padded[None],
            conv_taps[layer][:, None, :],
            (1,),
            "VALID",
            dimension_numbers=("NWC", "WIO", "NWC"),
            feature_group_count=local_ch,
            precision=lax.Precision.HIGHEST,
        )[0]
        mean = of_everyone(jnp.sum(conv, axis=1, keepdims=True), "tp") / C
        centred = conv - mean
        spread = of_everyone(jnp.sum(centred * centred, axis=1, keepdims=True), "tp") / C
        act = jax.nn.silu(centred * lax.rsqrt(spread + 1e-05) * channel_gain[layer]).astype(
            jnp.bfloat16
        )
        out_whole = gathered_by_axis(w_out[layer], (("sp_0", "sp_1"), "sp_2"), (0, 1), 1)
        terms = jnp.dot(act, out_whole, preferred_element_type=jnp.float32)
        branch = sum_at_owner(terms.astype(jnp.bfloat16), "tp", 1)
        x = (x.astype(jnp.float32) + branch).astype(jnp.bfloat16)
    return x


def solution(mesh):
    finer = Mesh(mesh.devices.reshape(8, 8, 2, mesh.shape["tp"]), ("sp_0", "sp_1", "sp_2", "tp"))
    in_specs = (
        P(SP, "tp"),
        P(),
        P(None, SP, "tp"),
        P(None, SP, "tp"),
        P(None, None, "tp"),
        P(None, "tp"),
        P(None, "tp", SP),
    )
    out_specs = P(SP, "tp")
    return jax.shard_map(
        shards, mesh=finer, in_specs=in_specs, out_specs=out_specs, check_vma=False
    )
```

profile of v0, /device:TPU:24, one launch (start us, length us, event | category | flops | bytes accessed | tf_op | source)
XLA Modules:
  0.0 303.7 jit_solution(6002797034493604324)
XLA Ops:
  6.5 0.7 slice_bitcast_fusion
  7.3 0.6 pad_maximum_fusion
  8.0 0.7 fusion.40
  8.7 60.0 %all_gather.19 = bf16[64,256,16]{1,2,0:T(8,128)(2,1)} all-gather(bf16[1,256,16]{1,2,0:T(8,128)(2,1)S(1)} %get-tuple-element.13), channel_id=1, replica_groups=mesh['sp_0'=8,'sp_1'=8,'sp_2'=2,'tp'=4] {'sp_0','sp_1'}, dimensions={0}, use_global_device_ids=true | all-gather | bytes 532480 | tf_op jit(solution)/shard_map/all_gather | solution.py:49
  68.7 1.1 copy.36
  69.8 1.1 broadcast_in_dim.30
  70.9 4.3 %all-to-all-start = ((bf16[4,256,512]{1,2,0:T(8,128)(2,1)}), bf16[4,256,512]{1,2,0:T(8,128)(2,1)S(1)}, u32[]{:S(2)}, u32[]{:S(2)}) async-start(bf16[4,256,512]{1,2,0:T(8,128)(2,1)} %broadcast_in_dim.30), calls=%async_computation | async-start | bytes 2097152 | tf_op jit(solution)/shard_map/all_to_all | solution.py:20
  75.2 0.6 pad_maximum_fusion.1
  75.8 0.1 all-gather.9.cloned.1.call-update
  75.9 10.1 %all-to-all-done = bf16[4,256,512]{1,2,0:T(8,128)(2,1)S(1)} async-done(((bf16[4,256,512]{1,2,0:T(8,128)(2,1)}), bf16[4,256,512]{1,2,0:T(8,128)(2,1)S(1)}, u32[]{:S(2)}, u32[]{:S(2)}) %all-to-all-start) | async-done | bytes 1048608 | tf_op jit(solution)/shard_map/all_to_all | solution.py:20
  86.0 0.3 multiply_reduce_fusion.1
  86.4 0.3 fusion.3
  86.7 11.0 %all-gather.5.cloned.1.call-done = bf16[2048,512]{1,0:T(8,128)(2,1)} async-done(((bf16[16,512]{1,0:T(8,128)(2,1)}), bf16[2048,512]{1,0:T(8,128)(2,1)}) %all-gather.5.cloned.1.call-update) | async-done | bytes 2097168 | tf_op jit(solution)/shard_map/all_gather | solution.py:29
  97.7 1.8 fusion.18
  99.6 0.5 fusion.12
  100.2 2.1 collective-permute-start
  102.3 3.4 %collective-permute-done = bf16[128,256]{1,0:T(8,128)(2,1)S(1)} collective-permute-done((bf16[128,256]{1,0:T(8,128)(2,1)S(1)}, bf16[128,256]{1,0:T(8,128)(2,1)S(1)}, u32[]{:S(2)}, u32[]{:S(2)}) %collective-permute-start) | collective-permute-done | bytes 65568 | tf_op jit(solution)/shard_map/ppermute | solution.py:39
  105.8 4.8 %fusion.42 = (f32[256]{0:T(256)S(1)}, f32[1,256,256]{2,0,1:T(1,128)S(1)}) fusion(f32[1,128,256]{2,1,0:T(8,128)S(1)} %get-tuple-element.6, bf16[1,383,256]{2,1,0:T(8,128)(2,1)S(1)} %maximum_bitcast_fusion), kind=kOutput, calls=%fused_computation.76 | convolution fusion | flops 100728576 | bytes 590336 | tf_op jit(solution)/shard_map/conv_general_dilated | solution.py:90
  110.7 9.2 %all_to_all.40 = f32[4,256,1]{1,2,0:T(1,128)S(1)} all-to-all(f32[4,256,1]{1,2,0:T(1,128)S(1)} %broadcast_in_dim.32), channel_id=1, replica_groups=mesh['sp_0'=8,'sp_1'=8,'sp_2'=2,'tp'=4] {'tp'}, dimensions={0} | all-to-all | bytes 8192 | tf_op jit(solution)/shard_map/all_to_all | solution.py:20
  119.9 0.2 fusion.27
  120.1 0.6 broadcast_in_dim.33
  120.7 3.2 %all-to-all-start.2 = ((f32[4,256,1]{1,2,0:T(1,128)}), f32[4,256,1]{1,2,0:T(1,128)S(1)}, u32[]{:S(2)}, u32[]{:S(2)}) async-start(f32[4,256,1]{1,2,0:T(1,128)} %broadcast_in_dim.33), calls=%async_computation.2 | async-start | bytes 8192 | tf_op jit(solution)/shard_map/all_to_all | solution.py:20
  124.1 1.4 copy.40
  125.4 3.8 %all-to-all-done.2 = f32[4,256,1]{1,2,0:T(1,128)S(1)} async-done(((f32[4,256,1]{1,2,0:T(1,128)}), f32[4,256,1]{1,2,0:T(1,128)S(1)}, u32[]{:S(2)}, u32[]{:S(2)}) %all-to-all-start.2) | async-done | bytes 4128 | tf_op jit(solution)/shard_map/all_to_all | solution.py:20
  129.3 0.5 convolution_convert_fusion.1
  129.8 0.1 copy.83
  129.9 15.3 %all_to_all.41 = bf16[4,256,512]{2,1,0:T(8,128)(2,1)S(1)} all-to-all(bf16[4,256,512]{2,1,0:T(8,128)(2,1)S(1)} %bitcast.96), channel_id=1, replica_groups=mesh['sp_0'=8,'sp_1'=8,'sp_2'=2,'tp'=4] {'tp'}, dimensions={0} | all-to-all | bytes 2097152 | tf_op jit(solution)/shard_map/all_to_all | solution.py:68
  145.1 0.1 convert_reduce_fusion.1
  145.4 0.1 copy.42
  145.6 14.3 %all_to_all.42 = bf16[4,256,512]{1,2,0:T(8,128)(2,1)S(1)} all-to-all(bf16[4,256,512]{1,2,0:T(8,128)(2,1)S(1)} %broadcast_in_dim.34), channel_id=1, replica_groups=mesh['sp_0'=8,'sp_1'=8,'sp_2'=2,'tp'=4] {'tp'}, dimensions={0} | all-to-all | bytes 2097152 | tf_op jit(solution)/shard_map/all_to_all | solution.py:20
  159.9 0.3 multiply_reduce_fusion
  160.2 0.3 fusion.1
  160.5 40.8 %all-gather.9.cloned.1.call-done = bf16[2048,512]{1,0:T(8,128)(2,1)} async-done(((bf16[16,512]{1,0:T(8,128)(2,1)}), bf16[2048,512]{1,0:T(8,128)(2,1)}) %all-gather.9.cloned.1.call-update) | async-done | bytes 2097168 | tf_op jit(solution)/shard_map/all_gather | solution.py:29
  201.3 1.8 fusion.15
  203.2 0.5 fusion.13
  203.7 2.1 collective-permute-start.1
  205.9 52.8 %all_gather.22 = bf16[64,256,16]{1,2,0:T(8,128)(2,1)} all-gather(bf16[1,256,16]{1,2,0:T(8,128)(2,1)S(1)} %get-tuple-element.14), channel_id=1, replica_groups=mesh['sp_0'=8,'sp_1'=8,'sp_2'=2,'tp'=4] {'sp_0','sp_1'}, dimensions={0}, use_global_device_ids=true | all-gather | bytes 532480 | tf_op jit(solution)/shard_map/all_gather | solution.py:49
  258.8 4.8 %fusion.43 = (f32[256]{0:T(256)S(1)}, f32[1,256,256]{2,0,1:T(1,128)S(1)}) fusion(f32[1,128,256]{2,1,0:T(8,128)S(1)} %get-tuple-element.5, bf16[1,383,256]{2,1,0:T(8,128)(2,1)S(1)} %maximum_bitcast_fusion.1), kind=kOutput, calls=%fused_computation.77 | convolution fusion | flops 100728576 | bytes 590336 | tf_op jit(solution)/shard_map/conv_general_dilated | solution.py:90
  263.6 9.3 %all_to_all.43 = f32[4,256,1]{1,2,0:T(1,128)S(1)} all-to-all(f32[4,256,1]{1,2,0:T(1,128)S(1)} %broadcast_in_dim.36), channel_id=1, replica_groups=mesh['sp_0'=8,'sp_1'=8,'sp_2'=2,'tp'=4] {'tp'}, dimensions={0} | all-to-all | bytes 8192 | tf_op jit(solution)/shard_map/all_to_all | solution.py:20
  273.0 0.2 fusion.25
  273.2 0.6 broadcast_in_dim.37
  273.8 3.2 %all-to-all-start.6 = ((f32[4,256,1]{1,2,0:T(1,128)}), f32[4,256,1]{1,2,0:T(1,128)S(1)}, u32[]{:S(2)}, u32[]{:S(2)}) async-start(f32[4,256,1]{1,2,0:T(1,128)} %broadcast_in_dim.37), calls=%async_computation.6 | async-start | bytes 8192 | tf_op jit(solution)/shard_map/all_to_all | solution.py:20
  277.1 1.4 copy.46
  278.4 3.9 %all-to-all-done.6 = f32[4,256,1]{1,2,0:T(1,128)S(1)} async-done(((f32[4,256,1]{1,2,0:T(1,128)}), f32[4,256,1]{1,2,0:T(1,128)S(1)}, u32[]{:S(2)}, u32[]{:S(2)}) %all-to-all-start.6) | async-done | bytes 4128 | tf_op jit(solution)/shard_map/all_to_all | solution.py:20
  282.3 0.5 convolution_convert_fusion
  282.9 13.3 %all_to_all.44 = bf16[4,256,512]{2,1,0:T(8,128)(2,1)S(1)} all-to-all(bf16[4,256,512]{2,1,0:T(8,128)(2,1)S(1)} %bitcast.97), channel_id=1, replica_groups=mesh['sp_0'=8,'sp_1'=8,'sp_2'=2,'tp'=4] {'tp'}, dimensions={0} | all-to-all | bytes 2097152 | tf_op jit(solution)/shard_map/all_to_all | solution.py:68
  296.2 0.1 convert_reduce_fusion
  296.4 0.8 add_convert_fusion
  (46 shorter events, 0.9 us)
Async XLA Ops:
  6.5 91.2 %all-gather.5.cloned.1.call-start = ((), (), s32[]{:S(2)}) async-start(), calls=%async_computation.8 | async-start | bytes 2113536 | tf_op jit(solution)/shard_map/all_gather | solution.py:29
  7.9 116.1 %all-gather.7.cloned.1.call-start = ((), (), s32[]{:S(2)}) async-start(), calls=%async_computation.9 | async-start | bytes 1572864 | tf_op jit(solution)/shard_map/all_gather | solution.py:49
  68.7 7.2 %copy-start.4 = (f32[2,2048]{1,0:T(2,128)S(1)}, f32[2,2048]{1,0:T(2,128)}, u32[]{:S(2)}) copy-start(f32[2,2048]{1,0:T(2,128)} %param.8) | copy-start | bytes 49156
  70.9 15.2 %all-to-all-start = ((bf16[4,256,512]{1,2,0:T(8,128)(2,1)}), bf16[4,256,512]{1,2,0:T(8,128)(2,1)S(1)}, u32[]{:S(2)}, u32[]{:S(2)}) async-start(bf16[4,256,512]{1,2,0:T(8,128)(2,1)} %broadcast_in_dim.30), calls=%async_computation | async-start | bytes 2097152 | tf_op jit(solution)/shard_map/all_to_all | solution.py:20
  75.2 126.2 %all-gather.9.cloned.1.call-start = ((), (), s32[]{:S(2)}) async-start(), calls=%async_computation.10 | async-start | bytes 2113536 | tf_op jit(solution)/shard_map/all_gather | solution.py:29
  97.7 1.9 copy-start.2
  99.6 2.7 copy-start.3
  100.2 5.6 %collective-permute-start = (bf16[128,256]{1,0:T(8,128)(2,1)S(1)}, bf16[128,256]{1,0:T(8,128)(2,1)S(1)}, u32[]{:S(2)}, u32[]{:S(2)}) collective-permute-start(bf16[128,256]{1,0:T(8,128)(2,1)S(1)} %slice.82), channel_id=1, source_target_pairs={{0,4},{4,8},{8,12},{12,16},{16,20},{20,24},{24,28},{28,32},{32,36}... | collective-permute-start | bytes 196616 | tf_op jit(solution)/shard_map/ppermute | solution.py:39
  105.8 18.2 %copy-start.5 = (f32[2,256]{1,0:T(2,128)S(1)}, f32[2,256]{1,0:T(2,128)}, u32[]{:S(2)}) copy-start(f32[2,256]{1,0:T(2,128)} %param.12) | copy-start | bytes 6148
  120.7 8.5 %all-to-all-start.2 = ((f32[4,256,1]{1,2,0:T(1,128)}), f32[4,256,1]{1,2,0:T(1,128)S(1)}, u32[]{:S(2)}, u32[]{:S(2)}) async-start(f32[4,256,1]{1,2,0:T(1,128)} %broadcast_in_dim.33), calls=%async_computation.2 | async-start | bytes 8192 | tf_op jit(solution)/shard_map/all_to_all | solution.py:20
  124.0 153.1 %all-gather.11.cloned.1.call-start = ((), (), s32[]{:S(2)}) async-start(), calls=%async_computation.11 | async-start | bytes 1572864 | tf_op jit(solution)/shard_map/all_gather | solution.py:49
  129.9 15.4 %copy-start = (bf16[256,512]{1,0:T(8,128)(2,1)S(1)}, bf16[256,512]{1,0:T(8,128)(2,1)}, u32[]{:S(2)}) copy-start(bf16[256,512]{1,0:T(8,128)(2,1)} %param.7) | copy-start | bytes 786436
  201.3 1.9 copy-start.1
  203.7 54.9 %collective-permute-start.1 = (bf16[128,256]{1,0:T(8,128)(2,1)S(1)}, bf16[128,256]{1,0:T(8,128)(2,1)S(1)}, u32[]{:S(2)}, u32[]{:S(2)}) collective-permute-start(bf16[128,256]{1,0:T(8,128)(2,1)S(1)} %slice.86), channel_id=1, source_target_pairs={{0,4},{4,8},{8,12},{12,16},{16,20},{20,24},{24,28},{28,32},{32,36}... | collective-permute-start | bytes 196616 | tf_op jit(solution)/shard_map/ppermute | solution.py:39
  273.8 8.5 %all-to-all-start.6 = ((f32[4,256,1]{1,2,0:T(1,128)}), f32[4,256,1]{1,2,0:T(1,128)S(1)}, u32[]{:S(2)}, u32[]{:S(2)}) async-start(f32[4,256,1]{1,2,0:T(1,128)} %broadcast_in_dim.37), calls=%async_computation.6 | async-start | bytes 8192 | tf_op jit(solution)/shard_map/all_to_all | solution.py:20
Sparse Core Ops, SparseCore 0:
  10.5 87.2 all-gather.4
  99.8 14.3 all-gather.6
  117.3 83.9 all-gather.8
  258.8 14.8 all-gather.10
where the time goes:
time: 304 us
  blocking collectives  174 us (57%)
  waiting for transfers between devices  73.2 us (24%)
  matrix products  15.4 us (5%)
  starting transfers between devices  15.1 us (5%)
  between operations  13.4 us (4%)
  local copies, waits for them, and re-layouts  8.17 us (3%)
  other arithmetic  4.21 us (1%)
    all_gather x2, blocking collectives, stacked_from(): parts = lax.all_gather(parts, axes[k], axis=0, tiled=True)  113 us
    all_gather x2, waiting for transfers between devices, in_one_piece(): whole, at, done = (lax.all_gather(both, axis, axis=dim, tiled=True), 0, [])  51.8 us
    all_to_all x3, blocking collectives, sent_to_all(): return lax.all_to_all(copies, axis, split_axis=0, concat_axis=0, tiled=True)  32.8 us
    all_to_all x2, blocking collectives, sum_at_owner(): lax.all_to_all(parts, axis, split_axis=0, concat_axis=0, tiled=True)  28.6 us
    all_to_all x3, waiting for transfers between devices, sent_to_all(): return lax.all_to_all(copies, axis, split_axis=0, concat_axis=0, tiled=True)  17.8 us
    all_to_all x3, starting transfers between devices, sent_to_all(): return lax.all_to_all(copies, axis, split_axis=0, concat_axis=0, tiled=True)  10.8 us
    conv_general_dilated x2, matrix products, shards(): lax.conv_general_dilated(padded[None], conv_taps[layer][:, None, :], (1,)...  9.67 us
  transfers between devices with their start and end apart: 9, of which 6 were waited for; matrix products, arithmetic and copies ran while one was open for 7% of the time, Pallas kernels for 0%

commit v1 on v0

--- a/solution.py
+++ b/solution.py
@@ -46,7 +46,9 @@
 def stacked_from(shard, axes, turns):
     parts = shard[None]
     for k in turns:
-        parts = lax.all_gather(parts, axes[k], axis=0, tiled=True)
+        parts = jnp.concatenate(
+            lax.all_to_all(jnp.stack([parts] * lax.axis_size(axes[k])), axes[k], 0, 0), axis=0
+        )
     held = [lax.axis_size(axes[k]) for k in reversed(turns)]
     parts = parts.reshape(*held, *shard.shape)
     turned = sorted(range(len(turns)), key=lambda place: turns[len(turns) - 1 - place])

time: 304 us -> 252 us (0.83)
  the two profiles are of different devices: /device:TPU:24 before, /device:TPU:8 now
where the time goes in v1:
time: 252 us; the launch traced here: 251 us
  waiting for transfers between devices  100 us (40%)
  starting transfers between devices  57 us (23%)
  blocking collectives  49.9 us (20%)
  matrix products  15.4 us (6%)
  between operations  13.8 us (5%)
  local copies, waits for them, and re-layouts  7.83 us (3%)
  other arithmetic  6.34 us (3%)
    all_gather x2, waiting for transfers between devices, in_one_piece(): whole, at, done = (lax.all_gather(both, axis, axis=dim, tiled=True), 0, [])  53.6 us
    all_to_all x4, starting transfers between devices, stacked_from(): lax.all_to_all(jnp.stack([parts] * lax.axis_size(axes[k])), axes[k], 0, 0)  34.5 us
    all_to_all x2, blocking collectives, sum_at_owner(): lax.all_to_all(parts, axis, split_axis=0, concat_axis=0, tiled=True)  34 us
    all_to_all x5, waiting for transfers between devices, sent_to_all(): return lax.all_to_all(copies, axis, split_axis=0, concat_axis=0, tiled=True)  32.9 us
    all_to_all x5, starting transfers between devices, sent_to_all(): return lax.all_to_all(copies, axis, split_axis=0, concat_axis=0, tiled=True)  18.3 us
    all_to_all x1, blocking collectives, sent_to_all(): return lax.all_to_all(copies, axis, split_axis=0, concat_axis=0, tiled=True)  15.8 us
    conv_general_dilated x2, matrix products, shards(): lax.conv_general_dilated(padded[None], conv_taps[layer][:, None, :], (1,)...  9.67 us
    ppermute x2, waiting for transfers between devices, from_behind(): lax.ppermute(value, axis, [(source, source + steps) for source in range(i...  7.5 us
  transfers between devices with their start and end apart: 13, of which 11 were waited for; matrix products, arithmetic and copies ran while one was open for 10% of the time, Pallas kernels for 0%

profile of v1, /device:TPU:8, one launch (start us, length us, event | category | flops | bytes accessed | tf_op | source)
XLA Modules:
  0.0 250.6 jit_solution(16076256389904985067)
XLA Ops:
  6.5 0.8 slice_bitcast_fusion.1
  7.3 0.6 pad_maximum_fusion.2
  7.9 1.1 copy.30
  9.0 1.1 broadcast_in_dim.30
  10.1 4.3 %all-to-all-start = ((bf16[4,256,512]{1,2,0:T(8,128)(2,1)}), bf16[4,256,512]{1,2,0:T(8,128)(2,1)S(1)}, u32[]{:S(2)}, u32[]{:S(2)}) async-start(bf16[4,256,512]{1,2,0:T(8,128)(2,1)} %broadcast_in_dim.30), calls=%async_computation | async-start | bytes 2097152 | tf_op jit(solution)/shard_map/all_to_all | solution.py:20
  14.4 0.6 pad_maximum_fusion.3
  15.2 14.3 %all-to-all-done = bf16[4,256,512]{1,2,0:T(8,128)(2,1)S(1)} async-done(((bf16[4,256,512]{1,2,0:T(8,128)(2,1)}), bf16[4,256,512]{1,2,0:T(8,128)(2,1)S(1)}, u32[]{:S(2)}, u32[]{:S(2)}) %all-to-all-start) | async-done | bytes 1048608 | tf_op jit(solution)/shard_map/all_to_all | solution.py:20
  29.5 0.9 stack.12
  30.3 16.6 %all-to-all-start.3 = ((bf16[64,1,256,16]{2,3,1,0:T(8,128)(2,1)}), bf16[64,1,256,16]{2,3,1,0:T(8,128)(2,1)S(1)}, u32[]{:S(2)}, u32[]{:S(2)}) async-start(bf16[64,1,256,16]{2,3,1,0:T(8,128)(2,1)} %stack.12), calls=%async_computation.3 | async-start | bytes 1048576 | tf_op jit(solution)/shard_map/all_to_all | solution.py:50
  47.2 0.3 fusion.3
  47.6 53.6 %all-gather.3.cloned.1.call-done = bf16[2048,512]{1,0:T(8,128)(2,1)} async-done(((bf16[16,512]{1,0:T(8,128)(2,1)}), bf16[2048,512]{1,0:T(8,128)(2,1)}) %all-gather.3.cloned.1.call-update) | async-done | bytes 2097168 | tf_op jit(solution)/shard_map/all_gather | solution.py:29
  101.2 1.8 fusion.18
  103.1 0.5 fusion.12
  103.6 2.1 collective-permute-start
  105.8 3.4 %collective-permute-done = bf16[128,256]{1,0:T(8,128)(2,1)S(1)} collective-permute-done((bf16[128,256]{1,0:T(8,128)(2,1)S(1)}, bf16[128,256]{1,0:T(8,128)(2,1)S(1)}, u32[]{:S(2)}, u32[]{:S(2)}) %collective-permute-start) | collective-permute-done | bytes 65568 | tf_op jit(solution)/shard_map/ppermute | solution.py:39
  109.2 4.8 %fusion.41 = (f32[256]{0:T(256)S(1)}, f32[1,256,256]{2,0,1:T(1,128)S(1)}) fusion(f32[1,128,256]{2,1,0:T(8,128)S(1)} %get-tuple-element.6, bf16[1,383,256]{2,1,0:T(8,128)(2,1)S(1)} %maximum_bitcast_fusion), kind=kOutput, calls=%fused_computation.79 | convolution fusion | flops 100728576 | bytes 590336 | tf_op jit(solution)/shard_map/conv_general_dilated | solution.py:92
  114.1 0.6 broadcast_in_dim.32
  114.7 4.2 %all-to-all-start.1 = ((f32[4,256,1]{1,2,0:T(1,128)}), f32[4,256,1]{1,2,0:T(1,128)S(1)}, u32[]{:S(2)}, u32[]{:S(2)}) async-start(f32[4,256,1]{1,2,0:T(1,128)} %broadcast_in_dim.32), calls=%async_computation.1 | async-start | bytes 8192 | tf_op jit(solution)/shard_map/all_to_all | solution.py:20
  118.9 1.1 pad_maximum_fusion
  120.0 4.2 %all-to-all-done.1 = f32[4,256,1]{1,2,0:T(1,128)S(1)} async-done(((f32[4,256,1]{1,2,0:T(1,128)}), f32[4,256,1]{1,2,0:T(1,128)S(1)}, u32[]{:S(2)}, u32[]{:S(2)}) %all-to-all-start.1) | async-done | bytes 4128 | tf_op jit(solution)/shard_map/all_to_all | solution.py:20
  124.2 3.6 %all-to-all-start.4 = ((bf16[2,64,256,16]{2,3,1,0:T(8,128)(2,1)}), bf16[2,64,256,16]{2,3,1,0:T(8,128)(2,1)S(1)}, u32[]{:S(2)}, u32[]{:S(2)}) async-start(bf16[2,64,256,16]{2,3,1,0:T(8,128)(2,1)} %pad_maximum_fusion), calls=%async_computation.4 | async-start | bytes 2097152 | tf_op jit(solution)/shard_map/all_to_all | solution.py:50
  128.0 1.9 all-to-all-done.4
  129.9 0.6 broadcast_in_dim.33
  130.5 3.2 %all-to-all-start.2 = ((f32[4,256,1]{1,2,0:T(1,128)}), f32[4,256,1]{1,2,0:T(1,128)S(1)}, u32[]{:S(2)}, u32[]{:S(2)}) async-start(f32[4,256,1]{1,2,0:T(1,128)} %broadcast_in_dim.33), calls=%async_computation.2 | async-start | bytes 8192 | tf_op jit(solution)/shard_map/all_to_all | solution.py:20
  133.9 5.1 %all-to-all-done.2 = f32[4,256,1]{1,2,0:T(1,128)S(1)} async-done(((f32[4,256,1]{1,2,0:T(1,128)}), f32[4,256,1]{1,2,0:T(1,128)S(1)}, u32[]{:S(2)}, u32[]{:S(2)}) %all-to-all-start.2) | async-done | bytes 4128 | tf_op jit(solution)/shard_map/all_to_all | solution.py:20
  139.1 0.5 convolution_convert_fusion.1
  139.7 17.1 %all_to_all.60 = bf16[4,256,512]{2,1,0:T(8,128)(2,1)S(1)} all-to-all(bf16[4,256,512]{2,1,0:T(8,128)(2,1)S(1)} %bitcast.100), channel_id=1, replica_groups=mesh['sp_0'=8,'sp_1'=8,'sp_2'=2,'tp'=4] {'tp'}, dimensions={0} | all-to-all | bytes 2097152 | tf_op jit(solution)/shard_map/all_to_all | solution.py:70
  157.2 15.8 %all_to_all.61 = bf16[4,256,512]{1,2,0:T(8,128)(2,1)S(1)} all-to-all(bf16[4,256,512]{1,2,0:T(8,128)(2,1)S(1)} %broadcast_in_dim.34), channel_id=1, replica_groups=mesh['sp_0'=8,'sp_1'=8,'sp_2'=2,'tp'=4] {'tp'}, dimensions={0} | all-to-all | bytes 2097152 | tf_op jit(solution)/shard_map/all_to_all | solution.py:20
  173.1 0.8 stack.14
  173.9 10.7 %all-to-all-start.9 = ((bf16[64,1,256,16]{2,3,1,0:T(8,128)(2,1)}), bf16[64,1,256,16]{2,3,1,0:T(8,128)(2,1)S(1)}, u32[]{:S(2)}, u32[]{:S(2)}) async-start(bf16[64,1,256,16]{2,3,1,0:T(8,128)(2,1)} %stack.14), calls=%async_computation.9 | async-start | bytes 1048576 | tf_op jit(solution)/shard_map/all_to_all | solution.py:50
  185.3 1.8 fusion.15
  187.2 0.5 fusion.13
  187.7 2.1 collective-permute-start.1
  189.9 4.1 %collective-permute-done.1 = bf16[128,256]{1,0:T(8,128)(2,1)S(1)} collective-permute-done((bf16[128,256]{1,0:T(8,128)(2,1)S(1)}, bf16[128,256]{1,0:T(8,128)(2,1)S(1)}, u32[]{:S(2)}, u32[]{:S(2)}) %collective-permute-start.1) | collective-permute-done | bytes 65568 | tf_op jit(solution)/shard_map/ppermute | solution.py:39
  194.0 4.8 %fusion.42 = (f32[256]{0:T(256)S(1)}, f32[1,256,256]{2,0,1:T(1,128)S(1)}) fusion(f32[1,128,256]{2,1,0:T(8,128)S(1)} %get-tuple-element.5, bf16[1,383,256]{2,1,0:T(8,128)(2,1)S(1)} %maximum_bitcast_fusion.1), kind=kOutput, calls=%fused_computation.80 | convolution fusion | flops 100728576 | bytes 590336 | tf_op jit(solution)/shard_map/conv_general_dilated | solution.py:92
  198.8 2.5 %all-to-all-done.9 = bf16[64,1,256,16]{2,3,1,0:T(8,128)(2,1)S(1)} async-done(((bf16[64,1,256,16]{2,3,1,0:T(8,128)(2,1)}), bf16[64,1,256,16]{2,3,1,0:T(8,128)(2,1)S(1)}, u32[]{:S(2)}, u32[]{:S(2)}) %all-to-all-start.9) | async-done | bytes 524320 | tf_op jit(solution)/shard_map/all_to_all | solution.py:50
  201.4 0.6 broadcast_in_dim.36
  201.9 3.2 %all-to-all-start.7 = ((f32[4,256,1]{1,2,0:T(1,128)}), f32[4,256,1]{1,2,0:T(1,128)S(1)}, u32[]{:S(2)}, u32[]{:S(2)}) async-start(f32[4,256,1]{1,2,0:T(1,128)} %broadcast_in_dim.36), calls=%async_computation.7 | async-start | bytes 8192 | tf_op jit(solution)/shard_map/all_to_all | solution.py:20
  205.2 1.1 pad_maximum_fusion.1
  206.3 4.2 %all-to-all-done.7 = f32[4,256,1]{1,2,0:T(1,128)S(1)} async-done(((f32[4,256,1]{1,2,0:T(1,128)}), f32[4,256,1]{1,2,0:T(1,128)S(1)}, u32[]{:S(2)}, u32[]{:S(2)}) %all-to-all-start.7) | async-done | bytes 4128 | tf_op jit(solution)/shard_map/all_to_all | solution.py:20
  210.5 3.6 %all-to-all-start.10 = ((bf16[2,64,256,16]{2,3,1,0:T(8,128)(2,1)}), bf16[2,64,256,16]{2,3,1,0:T(8,128)(2,1)S(1)}, u32[]{:S(2)}, u32[]{:S(2)}) async-start(bf16[2,64,256,16]{2,3,1,0:T(8,128)(2,1)} %pad_maximum_fusion.1), calls=%async_computation.10 | async-start | bytes 2097152 | tf_op jit(solution)/shard_map/all_to_all | solution.py:50
  214.3 1.9 all-to-all-done.10
  216.2 0.6 broadcast_in_dim.37
  216.7 3.2 %all-to-all-start.8 = ((f32[4,256,1]{1,2,0:T(1,128)}), f32[4,256,1]{1,2,0:T(1,128)S(1)}, u32[]{:S(2)}, u32[]{:S(2)}) async-start(f32[4,256,1]{1,2,0:T(1,128)} %broadcast_in_dim.37), calls=%async_computation.8 | async-start | bytes 8192 | tf_op jit(solution)/shard_map/all_to_all | solution.py:20
  220.1 5.1 %all-to-all-done.8 = f32[4,256,1]{1,2,0:T(1,128)S(1)} async-done(((f32[4,256,1]{1,2,0:T(1,128)}), f32[4,256,1]{1,2,0:T(1,128)S(1)}, u32[]{:S(2)}, u32[]{:S(2)}) %all-to-all-start.8) | async-done | bytes 4128 | tf_op jit(solution)/shard_map/all_to_all | solution.py:20
  225.3 0.5 convolution_convert_fusion
  225.9 16.9 %all_to_all.62 = bf16[4,256,512]{2,1,0:T(8,128)(2,1)S(1)} all-to-all(bf16[4,256,512]{2,1,0:T(8,128)(2,1)S(1)} %bitcast.101), channel_id=1, replica_groups=mesh['sp_0'=8,'sp_1'=8,'sp_2'=2,'tp'=4] {'tp'}, dimensions={0} | all-to-all | bytes 2097152 | tf_op jit(solution)/shard_map/all_to_all | solution.py:70
  243.0 0.8 add_convert_fusion
  (54 shorter events, 2.9 us)
Async XLA Ops:
  6.5 8.6 %copy-start.4 = (bf16[2,256,16]{1,2,0:T(8,128)(2,1)S(1)}, bf16[2,256,16]{1,2,0:T(8,128)(2,1)}, u32[]{:S(2)}) copy-start(bf16[2,256,16]{1,2,0:T(8,128)(2,1)} %param.13) | copy-start | bytes 49156
  6.5 8.6 %copy-start.5 = (f32[2,2048]{1,0:T(2,128)S(1)}, f32[2,2048]{1,0:T(2,128)}, u32[]{:S(2)}) copy-start(f32[2,2048]{1,0:T(2,128)} %param.8) | copy-start | bytes 49156
  6.5 94.6 %all-gather.3.cloned.1.call-start = ((), (), s32[]{:S(2)}) async-start(), calls=%async_computation.12 | async-start | bytes 2113536 | tf_op jit(solution)/shard_map/all_gather | solution.py:29
  10.1 19.4 %all-to-all-start = ((bf16[4,256,512]{1,2,0:T(8,128)(2,1)}), bf16[4,256,512]{1,2,0:T(8,128)(2,1)S(1)}, u32[]{:S(2)}, u32[]{:S(2)}) async-start(bf16[4,256,512]{1,2,0:T(8,128)(2,1)} %broadcast_in_dim.30), calls=%async_computation | async-start | bytes 2097152 | tf_op jit(solution)/shard_map/all_to_all | solution.py:20
  14.4 170.9 %all-gather.5.cloned.1.call-start = ((), (), s32[]{:S(2)}) async-start(), calls=%async_computation.13 | async-start | bytes 2113536 | tf_op jit(solution)/shard_map/all_gather | solution.py:29
  30.3 83.8 %all-to-all-start.3 = ((bf16[64,1,256,16]{2,3,1,0:T(8,128)(2,1)}), bf16[64,1,256,16]{2,3,1,0:T(8,128)(2,1)S(1)}, u32[]{:S(2)}, u32[]{:S(2)}) async-start(bf16[64,1,256,16]{2,3,1,0:T(8,128)(2,1)} %stack.12), calls=%async_computation.3 | async-start | bytes 1048576 | tf_op jit(solution)/shard_map/all_to_all | solution.py:50
  101.2 1.9 copy-start.2
  103.1 2.7 %copy-start.3 = (f32[2,128,256]{2,1,0:T(8,128)S(1)}, f32[2,128,256]{2,1,0:T(8,128)}, u32[]{:S(2)}) copy-start(f32[2,128,256]{2,1,0:T(8,128)} %param.11) | copy-start | bytes 786436
  103.6 5.6 %collective-permute-start = (bf16[128,256]{1,0:T(8,128)(2,1)S(1)}, bf16[128,256]{1,0:T(8,128)(2,1)S(1)}, u32[]{:S(2)}, u32[]{:S(2)}) collective-permute-start(bf16[128,256]{1,0:T(8,128)(2,1)S(1)} %slice.88), channel_id=1, source_target_pairs={{0,4},{4,8},{8,12},{12,16},{16,20},{20,24},{24,28},{28,32},{32,36}... | collective-permute-start | bytes 196616 | tf_op jit(solution)/shard_map/ppermute | solution.py:39
  114.1 19.7 %copy-start.6 = (f32[2,256]{1,0:T(2,128)S(1)}, f32[2,256]{1,0:T(2,128)}, u32[]{:S(2)}) copy-start(f32[2,256]{1,0:T(2,128)} %param.12) | copy-start | bytes 6148
  114.7 9.5 %all-to-all-start.1 = ((f32[4,256,1]{1,2,0:T(1,128)}), f32[4,256,1]{1,2,0:T(1,128)S(1)}, u32[]{:S(2)}, u32[]{:S(2)}) async-start(f32[4,256,1]{1,2,0:T(1,128)} %broadcast_in_dim.32), calls=%async_computation.1 | async-start | bytes 8192 | tf_op jit(solution)/shard_map/all_to_all | solution.py:20
  124.2 5.7 %all-to-all-start.4 = ((bf16[2,64,256,16]{2,3,1,0:T(8,128)(2,1)}), bf16[2,64,256,16]{2,3,1,0:T(8,128)(2,1)S(1)}, u32[]{:S(2)}, u32[]{:S(2)}) async-start(bf16[2,64,256,16]{2,3,1,0:T(8,128)(2,1)} %pad_maximum_fusion), calls=%async_computation.4 | async-start | bytes 2097152 | tf_op jit(solution)/shard_map/all_to_all | solution.py:50
  130.5 8.5 %all-to-all-start.2 = ((f32[4,256,1]{1,2,0:T(1,128)}), f32[4,256,1]{1,2,0:T(1,128)S(1)}, u32[]{:S(2)}, u32[]{:S(2)}) async-start(f32[4,256,1]{1,2,0:T(1,128)} %broadcast_in_dim.33), calls=%async_computation.2 | async-start | bytes 8192 | tf_op jit(solution)/shard_map/all_to_all | solution.py:20
  139.7 17.2 %copy-start = (bf16[256,512]{1,0:T(8,128)(2,1)S(1)}, bf16[256,512]{1,0:T(8,128)(2,1)}, u32[]{:S(2)}) copy-start(bf16[256,512]{1,0:T(8,128)(2,1)} %param.7) | copy-start | bytes 786436
  173.9 27.5 %all-to-all-start.9 = ((bf16[64,1,256,16]{2,3,1,0:T(8,128)(2,1)}), bf16[64,1,256,16]{2,3,1,0:T(8,128)(2,1)S(1)}, u32[]{:S(2)}, u32[]{:S(2)}) async-start(bf16[64,1,256,16]{2,3,1,0:T(8,128)(2,1)} %stack.14), calls=%async_computation.9 | async-start | bytes 1048576 | tf_op jit(solution)/shard_map/all_to_all | solution.py:50
  185.3 1.9 copy-start.1
  187.7 6.2 %collective-permute-start.1 = (bf16[128,256]{1,0:T(8,128)(2,1)S(1)}, bf16[128,256]{1,0:T(8,128)(2,1)S(1)}, u32[]{:S(2)}, u32[]{:S(2)}) collective-permute-start(bf16[128,256]{1,0:T(8,128)(2,1)S(1)} %slice.92), channel_id=1, source_target_pairs={{0,4},{4,8},{8,12},{12,16},{16,20},{20,24},{24,28},{28,32},{32,36}... | collective-permute-start | bytes 196616 | tf_op jit(solution)/shard_map/ppermute | solution.py:39
  201.9 8.5 %all-to-all-start.7 = ((f32[4,256,1]{1,2,0:T(1,128)}), f32[4,256,1]{1,2,0:T(1,128)S(1)}, u32[]{:S(2)}, u32[]{:S(2)}) async-start(f32[4,256,1]{1,2,0:T(1,128)} %broadcast_in_dim.36), calls=%async_computation.7 | async-start | bytes 8192 | tf_op jit(solution)/shard_map/all_to_all | solution.py:20
  210.5 5.7 %all-to-all-start.10 = ((bf16[2,64,256,16]{2,3,1,0:T(8,128)(2,1)}), bf16[2,64,256,16]{2,3,1,0:T(8,128)(2,1)S(1)}, u32[]{:S(2)}, u32[]{:S(2)}) async-start(bf16[2,64,256,16]{2,3,1,0:T(8,128)(2,1)} %pad_maximum_fusion.1), calls=%async_computation.10 | async-start | bytes 2097152 | tf_op jit(solution)/shard_map/all_to_all | solution.py:50
  216.7 8.5 %all-to-all-start.8 = ((f32[4,256,1]{1,2,0:T(1,128)}), f32[4,256,1]{1,2,0:T(1,128)S(1)}, u32[]{:S(2)}, u32[]{:S(2)}) async-start(f32[4,256,1]{1,2,0:T(1,128)} %broadcast_in_dim.37), calls=%async_computation.8 | async-start | bytes 8192 | tf_op jit(solution)/shard_map/all_to_all | solution.py:20
Sparse Core Ops, SparseCore 0:
  10.5 90.6 all-gather.2
  104.3 80.0 all-gather.4
